TPU v7x, 32 devices: a whole 2x2x4 slice. The times are simulated.
32 devices in a mesh: ep: 8 (over z, core), tp: 4 (over y, x).
Axes of the slice: x: 2, y: 2, z: 4, core: 2. Of those that a mesh axis runs over, the one named last changes fastest.
Arguments:
- mixer_value_input: bfloat16 [2048, 4096], P('ep', 'tp'), may hold values from -6 to 6
- input_state_matrix: bfloat16 [2048, 2048], P('ep', 'tp'), may hold values from -6 to 6
- output_state_matrix: bfloat16 [2048, 2048], P('ep', 'tp'), may hold values from -6 to 6
- output_gate_input: bfloat16 [2048, 4096], P('ep', 'tp'), may hold values from -6 to 6
- step_input: float32 [2048, 64], P('ep', 'tp'), may hold values from -6 to -2
- extra_log_decay: float32 [2048, 64], P('ep', 'tp'), may hold values from -1 to 0
- head_log_decay: float32 [64], P('tp'), may hold values from -10 to 1
- head_skip_scale: float32 [64], P('tp'), may hold values from 0.5 to 2
- value_kernel: float32 [4, 4096], P(None, 'tp'), may hold values from -3 to 3
- input_matrix_kernel: float32 [4, 2048], P(None, 'tp'), may hold values from -3 to 3
- output_matrix_kernel: float32 [4, 2048], P(None, 'tp'), may hold values from -3 to 3
- mixer_norm_scale: float32 [4096], P('tp'), may hold values from 0.1 to 1.9
- mixer_output_weight: bfloat16 [4096, 2048], P(None, 'tp'), may hold values from -0.09375 to 0.09375
- second_token_rows: bfloat16 [2048, 2048], P('ep'), may hold values from -6 to 6
- expert_norm_scale: float32 [2048], replicated, may hold values from 0.1 to 1.9
- routed_expert_index: int32 [2048, 4], P('ep'), may hold values from 0 to 15, all different within a row; in each aligned block of 256 rows (0 to 255, 256 to 511, ...) at most 96 rows name the same one
- routed_expert_weight: float32 [2048, 4], P('ep'), may hold values from 0.1 to 1
- routed_gate_weight: bfloat16 [16, 2048, 1024], P('ep', None, 'tp'), may hold values from -0.125 to 0.125
- routed_up_weight: bfloat16 [16, 2048, 1024], P('ep', None, 'tp'), may hold values from -0.125 to 0.125
- routed_down_weight: bfloat16 [16, 1024, 2048], P('ep', None, 'tp'), may hold values from -0.1875 to 0.1875
- shared_gate_weight: bfloat16 [2048, 1024], P(None, 'tp'), may hold values from -0.125 to 0.125
- shared_up_weight: bfloat16 [2048, 1024], P(None, 'tp'), may hold values from -0.125 to 0.125
- shared_down_weight: bfloat16 [1024, 2048], P(None, 'tp'), may hold values from -0.1875 to 0.1875
Outputs:
- mixer_output: bfloat16 [2048, 2048], P('ep', 'tp')
- routed_out: bfloat16 [2048, 2048], P('ep', 'tp')
Inputs may be any that keep to these rules, and one draw needn't show every extreme that they name: `routed_expert_index`: in each aligned block of 256 rows (the rows of one index of ep) no expert is named more than 96 times, a bound that some block reaches.
All inputs are finite; a program needn't handle non-finite values.
Results may differ from a plain program's by a relative error of at most 0.012.
Values may be sent and summed in bfloat16 or wider, within the bound.
A program may use at most 64 MiB of HBM per device.

v0:
```python
import jax
import jax.numpy as jnp
from jax import lax
from jax.sharding import PartitionSpec as P

HEAD_DIM = 64
STATE = 128
CONV_TAPS = 4
BLOCK = 128
TOP_K = 4
epsilon = 1e-05
precise = lax.Precision.HIGHEST


def passed_along(x, axis, by):
    size = lax.axis_size(axis)
    pairs = [(i, i + by) for i in range(size) if 0 <= i + by < size]
    return lax.ppermute(x, axis, pairs)


def carried_in(x, axis, join, neutral):
    place = lax.axis_index(axis)
    gathered = jax.tree.map(
        lambda a, kind: lax.all_gather(a.astype(kind), axis), x, (jnp.bfloat16, jnp.bfloat16)
    )
    state = jax.tree.map(lambda a, e: jnp.zeros_like(a) + jnp.asarray(e, a.dtype), x, neutral)

    def one(turn, state):
        return join(
            state,
            jax.tree.map(
                lambda a, own: lax.dynamic_index_in_dim(a, turn, 0, False).astype(own.dtype),
                gathered,
                x,
            ),
        )

    return lax.fori_loop(0, place, one, state)


def conv_silu(tail_rows, source, weights):
    length = source.shape[0]
    padded = jnp.concatenate([tail_rows, source], axis=0)
    total_sum = jnp.zeros(source.shape, jnp.float32)
    for tap_index in range(CONV_TAPS):
        total_sum = (
            total_sum
            + padded[tap_index : tap_index + length].astype(jnp.float32) * weights[tap_index]
        )
    return jax.nn.silu(total_sum).astype(jnp.bfloat16)


def join_states(earlier, later_part):
    return (earlier[0] * later_part[0], later_part[0][:, None, None] * earlier[1] + later_part[1])


def carry_blocks(carried, inputs):
    block_decay, block_state = inputs
    return (carried * block_decay[:, None, None] + block_state, carried)


def route_slots(route_block, experts, capacity):
    flat_ids = route_block.reshape(-1)
    onehot = (flat_ids[:, None] == jnp.arange(experts, dtype=jnp.int32)[None, :]).astype(jnp.int32)
    earlier = jnp.cumsum(onehot, axis=0) - onehot
    position_in = jnp.sum(earlier * onehot, axis=1)
    slot_index = flat_ids * capacity + position_in
    owner_row = jnp.arange(flat_ids.shape[0], dtype=jnp.int32) // route_block.shape[1]
    slot_owner = (
        jnp.full((experts * capacity,), route_block.shape[0], jnp.int32)
        .at[slot_index]
        .set(owner_row)
    )
    return (slot_owner, slot_index)


def on_device(
    mixer_value_input,
    input_state_matrix,
    output_state_matrix,
    output_gate_input,
    step_input,
    extra_log_decay,
    head_log_decay,
    head_skip_scale,
    value_kernel,
    input_matrix_kernel,
    output_matrix_kernel,
    mixer_norm_scale,
    mixer_output_weight,
    second_token_rows,
    expert_norm_scale,
    routed_expert_index,
    routed_expert_weight,
    routed_gate_weight,
    routed_up_weight,
    routed_down_weight,
    shared_gate_weight,
    shared_up_weight,
    shared_down_weight,
):
    length = mixer_value_input.shape[0]
    heads_local = step_input.shape[1]
    width_x = mixer_value_input.shape[1]
    width_b = input_state_matrix.shape[1]
    groups_local = width_b // STATE
    head_ratio = heads_local // groups_local
    nblocks = length // BLOCK
    lead_row = length - CONV_TAPS + 1
    edge_rows = jnp.concatenate(
        [
            mixer_value_input[lead_row:],
            input_state_matrix[lead_row:],
            output_state_matrix[lead_row:],
        ],
        axis=1,
    )
    tail_rows = passed_along(edge_rows, "ep", 1)
    values = conv_silu(tail_rows[:, :width_x], mixer_value_input, value_kernel)
    in_mat = conv_silu(
        tail_rows[:, width_x : width_x + width_b], input_state_matrix, input_matrix_kernel
    )
    out_mat = conv_silu(
        tail_rows[:, width_x + width_b :], output_state_matrix, output_matrix_kernel
    )
    step_length = jax.nn.softplus(step_input)
    decay_logarithm = -jnp.exp(head_log_decay)[None, :] * step_length + extra_log_decay
    running = jnp.cumsum(decay_logarithm.reshape(nblocks, BLOCK, heads_local), axis=1)
    value_wide = values.astype(jnp.float32).reshape(nblocks, BLOCK, heads_local, HEAD_DIM)
    scaled = value_wide * step_length.reshape(nblocks, BLOCK, heads_local)[..., None]
    in_blocks = in_mat.reshape(nblocks, BLOCK, groups_local, STATE)
    out_blocks = out_mat.reshape(nblocks, BLOCK, groups_local, STATE)
    scores = jnp.einsum(
        "bign,bjgn->bgij", out_blocks, in_blocks, preferred_element_type=jnp.float32
    )
    scores = jnp.repeat(scores, head_ratio, axis=1)
    spread = jnp.transpose(running[:, :, None, :] - running[:, None, :, :], (0, 3, 1, 2))
    lower_mask = jnp.tril(jnp.ones((BLOCK, BLOCK), bool))[None, None]
    decay_mat = jnp.where(lower_mask, jnp.exp(jnp.where(lower_mask, spread, 0.0)), 0.0)
    inside = jnp.einsum("bhij,bjhp->bihp", scores * decay_mat, scaled, precision=precise)
    out_head = jnp.repeat(out_blocks.astype(jnp.float32), head_ratio, axis=2)
    in_head = jnp.repeat(in_blocks.astype(jnp.float32), head_ratio, axis=2)
    block_logs = running[:, -1]
    to_end = jnp.exp(block_logs[:, None, :] - running)
    block_state = jnp.einsum("bjhn,bjh,bjhp->bhpn", in_head, to_end, scaled, precision=precise)
    start_state = jnp.zeros((heads_local, HEAD_DIM, STATE), jnp.float32)
    local_total, local_prev = lax.scan(
        carry_blocks, start_state, (jnp.exp(block_logs), block_state)
    )
    before_logs = jnp.cumsum(block_logs, axis=0) - block_logs
    incoming = carried_in(
        (jnp.exp(jnp.sum(block_logs, axis=0)), local_total),
        "ep",
        join_states,
        (jnp.ones((heads_local,), jnp.float32), start_state),
    )
    entering = local_prev + jnp.exp(before_logs)[:, :, None, None] * incoming[1][None]
    carried_term = (
        jnp.einsum("bihn,bhpn->bihp", out_head, entering, precision=precise)
        * jnp.exp(running)[..., None]
    )
    mixed_heads = (inside + carried_term).reshape(length, heads_local, HEAD_DIM)
    mixed_heads = mixed_heads + head_skip_scale[None, :, None] * value_wide.reshape(
        length, heads_local, HEAD_DIM
    )
    gated_heads = mixed_heads * jax.nn.silu(output_gate_input.astype(jnp.float32)).reshape(
        length, heads_local, HEAD_DIM
    )
    grouped = gated_heads.reshape(length, groups_local, head_ratio * HEAD_DIM)
    grouped = grouped * lax.rsqrt(jnp.mean(grouped * grouped, axis=-1, keepdims=True) + epsilon)
    mixer_normed = (grouped.reshape(length, width_x) * mixer_norm_scale).astype(jnp.bfloat16)
    rows_local = second_token_rows.shape[0]
    model_width = second_token_rows.shape[1]
    local_experts = routed_gate_weight.shape[0]
    ep_count = lax.axis_size("ep")
    experts = local_experts * ep_count
    capacity = max(2, 3 * rows_local * TOP_K // (2 * experts))
    col_width = model_width // lax.axis_size("tp")
    rows_wide = second_token_rows.astype(jnp.float32)
    normed = (
        rows_wide
        * lax.rsqrt(jnp.mean(rows_wide * rows_wide, axis=-1, keepdims=True) + epsilon)
        * expert_norm_scale
    ).astype(jnp.bfloat16)
    slot_owner, slot_index = route_slots(routed_expert_index, experts, capacity)
    padded = jnp.concatenate([normed, jnp.zeros((1, model_width), jnp.bfloat16)], axis=0)
    outgoing = jnp.take(padded, slot_owner, axis=0).reshape(experts, capacity, model_width)
    my_columns = lax.dynamic_slice_in_dim(outgoing, lax.axis_index("tp") * col_width, col_width, 2)
    arrived = lax.all_to_all(my_columns, "ep", split_axis=0, concat_axis=1, tiled=True)
    column_piece = lax.all_gather(arrived, "tp", axis=2, tiled=True)
    gate_pre = jnp.einsum(
        "esd,edf->esf", column_piece, routed_gate_weight, preferred_element_type=jnp.float32
    )
    up_pre = jnp.einsum(
        "esd,edf->esf", column_piece, routed_up_weight, preferred_element_type=jnp.float32
    )
    hidden = (jax.nn.silu(gate_pre) * up_pre).astype(jnp.bfloat16)
    shared_hidden = (
        jax.nn.silu(jnp.dot(normed, shared_gate_weight, preferred_element_type=jnp.float32))
        * jnp.dot(normed, shared_up_weight, preferred_element_type=jnp.float32)
    ).astype(jnp.bfloat16)
    whole_mix, whole_hidden, whole_shared = (
        lax.all_gather(mixer_normed, "tp", axis=1, tiled=True),
        lax.all_gather(hidden, "tp", axis=2, tiled=True),
        lax.all_gather(shared_hidden, "tp", axis=1, tiled=True),
    )
    mixer_output = jnp.dot(
        whole_mix, mixer_output_weight, preferred_element_type=jnp.float32
    ).astype(jnp.bfloat16)
    expert_result = jnp.einsum(
        "esf,efd->esd", whole_hidden, routed_down_weight, preferred_element_type=jnp.float32
    ).astype(jnp.bfloat16)
    returned = lax.all_to_all(expert_result, "ep", split_axis=1, concat_axis=0, tiled=True)
    picked = jnp.take(returned.reshape(experts * capacity, col_width), slot_index, axis=0)
    picked = picked.reshape(rows_local, TOP_K, col_width).astype(jnp.float32)
    routed_sum = jnp.sum(picked * routed_expert_weight[:, :, None], axis=1)
    shared_result = jnp.dot(whole_shared, shared_down_weight, preferred_element_type=jnp.float32)
    routed_out = (routed_sum + shared_result).astype(jnp.bfloat16)
    return (mixer_output, routed_out)


def solution(mesh):
    return jax.shard_map(
        on_device,
        mesh=mesh,
        in_specs=(
            P("ep", "tp"),
            P("ep", "tp"),
            P("ep", "tp"),
            P("ep", "tp"),
            P("ep", "tp"),
            P("ep", "tp"),
            P("tp"),
            P("tp"),
            P(None, "tp"),
            P(None, "tp"),
            P(None, "tp"),
            P("tp"),
            P(None, "tp"),
            P("ep", None),
            P(),
            P("ep", None),
            P("ep", None),
            P("ep", None, "tp"),
            P("ep", None, "tp"),
            P("ep", None, "tp"),
            P(None, "tp"),
            P(None, "tp"),
            P(None, "tp"),
        ),
        out_specs=(P("ep", "tp"), P("ep", "tp")),
        check_vma=False,
    )
```

profile of v0, /device:TPU:0, one launch (start us, length us, event | category | flops | bytes accessed | tf_op | source)
XLA Modules:
  0.0 292.6 jit_solution(14076036180507357092)
XLA Ops:
  9.2 4.5 %reduce-window.6 = s32[16,8,128]{2,1,0:T(8,128)S(1)} reduce-window(s32[16,8,128]{2,1,0:T(8,128)S(1)} %fusion.50, s32[]{:T(128)} %constant.114.clone.1), window={size=1x1x128 pad=0_0x0_0x127_0}, to_apply=%region_8.9 | reduce-window | flops 2080768 | bytes 131076 | tf_op jit(solution)/shard_map/reduce-window
  15.6 4.3 %scatter_custom_fusion = s32[1536]{0:T(1024)S(1)} fusion(s32[1024]{0:T(1024)S(1)} %bitcast.142, s32[1024]{0:T(1024)S(1)} %add_select_fusion, s32[]{:T(128)} %constant.122.clone.1), kind=kCustom, calls=%fused_computation.105 | custom fusion | bytes 6148 | tf_op jit(solution)/shard_map/scatter | solution.py:72
  21.7 7.0 %gather_fusion = bf16[1536,2048]{1,0:T(8,128)(2,1)} fusion(bf16[257,2048]{1,0:T(8,128)(2,1)S(1)} %concatenate.19, s32[2048]{0:T(1024)S(1)} %pad_clamp_fusion), kind=kCustom, calls=%fused_computation | custom fusion | bytes 12589056 | tf_op jit(solution)/shard_map/jit(_take)/gather | solution.py:187
  30.6 43.9 %all_to_all.33 = bf16[16,96,512]{2,1,0:T(8,128)(2,1)S(1)} all-to-all(bf16[16,96,512]{2,1,0:T(8,128)(2,1)S(1)} %dynamic-slice_select_fusion), channel_id=1, replica_groups=mesh['ep'=8,'tp'=4] {'ep'}, dimensions={0} | all-to-all | bytes 3145728 | tf_op jit(solution)/shard_map/all_to_all | solution.py:189
  95.4 2.9 broadcast_multiply_fusion
  98.5 3.1 %fusion.26 = f32[2,16,64,128]{3,2,1,0:T(8,128)} fusion(f32[2,128,16,128]{3,1,2,0:T(8,128)S(1)} %bitcast.125, f32[2,128,16,64]{1,0,3,2:T(2,128)S(1)} %get-tuple-element.115), kind=kOutput, calls=%fused_computation.43 | convolution fusion | flops 402653184 | bytes 4194304 | tf_op jit(solution)/shard_map/bjhn,bjh,bjhp->bhpn/dot_general | solution.py:145
  101.6 4.1 %while.26 = (s32[]{:T(128)}, f32[16,64,128]{2,1,0:T(8,128)S(1)}, f32[2,16,64,128]{3,2,1,0:T(8,128)}, f32[2,16]{1,0:T(2,128)S(1)}, f32[2,16,64,128]{3,2,1,0:T(8,128)}, /*index=5*/s32[]{:T(128)}, s32[]{:T(128)}) while((s32[]{:T(128)}, f32[16,64,128]{2,1,0:T(8,128)S(1)}, f32[2,16,64,128]{3,2,1,0:T(8,128)}, f32[2,16]{1,0:T(2,128)S(1)}, ...), condition=%wide.region_2.3_spmd.clone, body=%wide.region_1.2_spmd.clone.sunk | while | flops 524291 | bytes 2622240 | solution.py:147
  106.7 38.1 %all-gather.9.cloned.1.call-done = bf16[2,768,2048]{2,1,0:T(8,128)(2,1)} async-done(((bf16[2,768,512]{2,1,0:T(8,128)(2,1)}), bf16[2,768,2048]{2,1,0:T(8,128)(2,1)}) %all-gather.9.cloned.1.call-update) | async-done | bytes 6291472 | tf_op jit(solution)/shard_map/all_gather | solution.py:190
  144.8 5.3 %fusion.62 = f32[2,768,256]{2,1,0:T(8,128)S(1)} fusion(bf16[2,768,2048]{2,1,0:T(8,128)(2,1)} %all-gather.9.cloned.1.call-done, bf16[2,2048,256]{2,1,0:T(8,128)(2,1)} %param.44), kind=kOutput, calls=%fused_computation.123 | convolution fusion | flops 1610612736 | bytes 9961472 | tf_op jit(solution)/shard_map/esd,edf->esf/dot_general | solution.py:191
  150.7 2.9 multiply_convert_fusion
  157.3 17.1 %all-reduce.1 = bf16[128]{0:T(256)(128)(2,1)S(1)} all-reduce(bf16[128]{0:T(256)(128)(2,1)S(1)} %dynamic-update-slice), channel_id=2, replica_groups=mesh['ep'=8,'tp'=4] {'ep'}, use_global_device_ids=true, to_apply=%add.1 | all-reduce | flops 128 | bytes 512
  181.6 4.2 %fusion.16 = f32[2,128,16,64]{1,3,2,0:T(8,128)S(1)} fusion(f32[2,128,16,128]{3,1,2,0:T(8,128)S(1)} %bitcast.126, f32[2,16,64,128]{3,2,1,0:T(8,128)S(1)} %copy-done.9, f32[2,128,16]{1,2,0:T(8,128)S(1)} %copy-done.14, f32[16,64,128]{2,1,0:T(8,128)S(1)} %get-tuple-element.76, f32[2,16]{1,0:T(2,128)S(1)} %copy-done.33), kind=kOutput, calls=%fused_computation.27 | convolution fusion | flops 403439616 | bytes 4735104 | tf_op jit(solution)/shard_map/bihn,bhpn->bihp/dot_general | solution.py:159
  187.1 4.2 %fusion.13 = f32[2,128,16,64]{1,3,2,0:T(8,128)S(1)} fusion(f32[2,128,16,64]{1,3,2,0:T(8,128)S(1)} %fusion.16, f32[2,16,128,128]{3,2,1,0:T(8,128)S(1)} %bitcast.124, f32[2,128,16,64]{1,0,3,2:T(2,128)S(1)} %copy-done.6, f32[2,16,128]{2,1,0:T(8,128)S(1)} %copy.106, pred[128,128]{1,0:T(8,128)(4,1)S(1)} %copy-done.13), kind=kOutput, calls=%fused_computation.25 | convolution fusion | flops 405012480 | bytes 5275648 | tf_op jit(solution)/shard_map/bhij,bjhp->bihp/dot_general | solution.py:140
  193.1 3.1 %reshape.204 = f32[256,4,256]{0,2,1:T(8,128)} reshape(f32[2,128,16,64]{1,0,3,2:T(2,128)} %copy.114) | data formatting | bytes 2097152 | tf_op jit(solution)/shard_map/reshape | solution.py:162
  199.6 21.9 %all-gather.11.cloned.1.call-done = bf16[2,768,1024]{2,1,0:T(8,128)(2,1)} async-done(((bf16[2,768,256]{2,1,0:T(8,128)(2,1)}), bf16[2,768,1024]{2,1,0:T(8,128)(2,1)}) %all-gather.11.cloned.1.call-update) | async-done | bytes 3145744 | tf_op jit(solution)/shard_map/all_gather | solution.py:204
  221.5 3.7 %convolution_convert_fusion = bf16[2,768,512]{2,1,0:T(8,128)(2,1)S(1)} fusion(bf16[2,768,1024]{2,1,0:T(8,128)(2,1)} %all-gather.11.cloned.1.call-done, bf16[2,1024,512]{2,1,0:T(8,128)(2,1)S(1)} %copy-done), kind=kOutput, calls=%fused_computation.21 | convolution fusion | flops 1611399168 | bytes 6815744 | tf_op jit(solution)/shard_map/esf,efd->esd/dot_general | solution.py:210
  227.9 5.0 %all-to-all-start.1 = ((bf16[2,768,512]{2,0,1:T(2,128)(2,1)}), bf16[2,768,512]{2,0,1:T(2,128)(2,1)}, u32[]{:S(2)}, u32[]{:S(2)}) async-start(bf16[2,768,512]{2,0,1:T(2,128)(2,1)} %copy.125), calls=%async_computation.1 | async-start | bytes 3145728 | tf_op jit(solution)/shard_map/all_to_all | solution.py:213
  235.7 20.6 %all_gather.28 = bf16[256,1024]{1,0:T(8,128)(2,1)} all-gather(bf16[256,256]{1,0:T(8,128)(2,1)S(1)} %fusion.18), channel_id=1, replica_groups=mesh['ep'=8,'tp'=4] {'tp'}, dimensions={1}, use_global_device_ids=true | all-gather | bytes 655360 | tf_op jit(solution)/shard_map/all_gather | solution.py:205
  256.3 6.2 %all-gather.7.cloned.1.call-done = bf16[256,4096]{0,1:T(8,128)(2,1)} async-done(((bf16[256,1024]{0,1:T(8,128)(2,1)}), bf16[256,4096]{0,1:T(8,128)(2,1)}) %all-gather.7.cloned.1.call-update) | async-done | bytes 2097168 | tf_op jit(solution)/shard_map/all_gather | solution.py:203
  262.6 4.8 %convolution_convert_fusion.1 = bf16[256,512]{1,0:T(8,128)(2,1)} fusion(bf16[256,4096]{0,1:T(8,128)(2,1)} %all-gather.7.cloned.1.call-done, bf16[4096,512]{1,0:T(8,128)(2,1)} %param.39), kind=kOutput, calls=%fused_computation.32 | convolution fusion | flops 1073872896 | bytes 6553600 | tf_op jit(solution)/shard_map/dot_general | solution.py:207
  267.3 3.5 %all-to-all-done.1 = bf16[2,768,512]{2,0,1:T(2,128)(2,1)} async-done(((bf16[2,768,512]{2,0,1:T(2,128)(2,1)}), bf16[2,768,512]{2,0,1:T(2,128)(2,1)}, u32[]{:S(2)}, u32[]{:S(2)}) %all-to-all-start.1) | async-done | bytes 1572896 | tf_op jit(solution)/shard_map/all_to_all | solution.py:213
  270.8 2.9 copy.126
  273.7 5.6 %gather_fusion.1 = bf16[1024,512]{1,0:T(8,128)(2,1)S(1)} fusion(bf16[1536,512]{1,0:T(8,128)(2,1)} %bitcast.121, s32[1024]{0:T(1024)S(1)} %broadcast_clamp_fusion), kind=kCustom, calls=%fused_computation.1 | custom fusion | bytes 2101248 | tf_op jit(solution)/shard_map/jit(_take)/gather | solution.py:214
  280.4 3.4 %multiply_reduce_fusion = f32[256,512]{1,0:T(8,128)S(1)} fusion(f32[256,4]{1,0:T(8,128)S(1)} %copy.127, bf16[256,4,512]{2,1,0:T(4,128)(2,1)} %gather.15, pred[256,4]{1,0:T(8,128)(4,1)S(1)} %copy.122), kind=kLoop, calls=%fused_computation.14 | loop fusion | flops 1966080 | bytes 1577984 | tf_op jit(solution)/shard_map/reduce_sum | solution.py:216
  (193 shorter events, 59.1 us)
Async XLA Ops:
  7.2 214.3 %copy-start = (bf16[2,1024,512]{2,1,0:T(8,128)(2,1)S(1)}, bf16[2,1024,512]{2,1,0:T(8,128)(2,1)}, u32[]{:S(2)}) copy-start(bf16[2,1024,512]{2,1,0:T(8,128)(2,1)} %param.46) | copy-start | bytes 6291460
  7.2 12.8 %copy-start.7 = (bf16[256,2048]{1,0:T(8,128)(2,1)S(1)}, bf16[256,2048]{1,0:T(8,128)(2,1)}, u32[]{:S(2)}) copy-start(bf16[256,2048]{1,0:T(8,128)(2,1)} %param.40) | copy-start | bytes 3145732
  7.2 13.2 %copy-start.25 = (f32[2048]{0:T(1024)S(1)}, f32[2048]{0:T(1024)}, u32[]{:S(2)}) copy-start(f32[2048]{0:T(1024)} %param.41) | copy-start | bytes 24580
  7.2 137.6 %all-gather.9.cloned.1.call-start = ((), (), s32[]{:S(2)}) async-start(), calls=%async_computation.3 | async-start | bytes 7864320 | tf_op jit(solution)/shard_map/all_gather | solution.py:190
  74.5 6.0 %copy-start.40 = (f32[16]{0:T(128)S(1)}, f32[16]{0:T(128)}, u32[]{:S(2)}) copy-start(f32[16]{0:T(128)} %param.33) | copy-start | bytes 196
  74.5 6.0 %copy-start.23 = (f32[256,16]{0,1:T(8,128)S(1)}, f32[256,16]{0,1:T(8,128)}, u32[]{:S(2)}) copy-start(f32[256,16]{0,1:T(8,128)} %param.31) | copy-start | bytes 49156
  74.5 6.0 %copy-start.24 = (f32[256,16]{0,1:T(8,128)S(1)}, f32[256,16]{0,1:T(8,128)}, u32[]{:S(2)}) copy-start(f32[256,16]{0,1:T(8,128)} %param.32) | copy-start | bytes 49156
  75.8 6.3 %copy-start.30 = (f32[4,512]{1,0:T(4,128)S(1)}, f32[4,512]{1,0:T(4,128)}, u32[]{:S(2)}) copy-start(f32[4,512]{1,0:T(4,128)} %param.36) | copy-start | bytes 24580
  75.8 6.9 %copy-start.22 = (f32[4,1024]{1,0:T(4,128)S(1)}, f32[4,1024]{1,0:T(4,128)}, u32[]{:S(2)}) copy-start(f32[4,1024]{1,0:T(4,128)} %param.35) | copy-start | bytes 49156
  75.8 104.3 %all-gather.13.cloned.1.call-start = ((), (), s32[]{:S(2)}) async-start(), calls=%async_computation.5 | async-start | bytes 2359296 | tf_op jit(solution)/shard_map/all_gather | solution.py:24
  78.4 7.2 %collective-permute-start = (bf16[3,2048]{0,1:T(8,128)(2,1)}, bf16[3,2048]{0,1:T(8,128)(2,1)}, u32[]{:S(2)}, u32[]{:S(2)}) collective-permute-start(bf16[3,2048]{0,1:T(8,128)(2,1)} %copy.98), channel_id=1, source_target_pairs={{0,4},{4,8},{8,12},{12,16},{16,20},{20,24},{24,28},{1,5},{5,9},{9,... | collective-permute-start | bytes 36872 | tf_op jit(solution)/shard_map/ppermute | solution.py:18
  106.5 115.0 %all-gather.11.cloned.1.call-start = ((), (), s32[]{:S(2)}) async-start(), calls=%async_computation.4 | async-start | bytes 3932160 | tf_op jit(solution)/shard_map/all_gather | solution.py:204
  144.8 5.4 %copy-start.37 = (bf16[2,768,2048]{2,1,0:T(8,128)(2,1)S(1)}, bf16[2,768,2048]{2,1,0:T(8,128)(2,1)}, u32[]{:S(2)}) copy-start(bf16[2,768,2048]{2,1,0:T(8,128)(2,1)} %all-gather.9.cloned.1.call-done) | copy-start | bytes 18874372
  144.8 5.8 %copy-start.38 = (bf16[2,2048,256]{2,1,0:T(8,128)(2,1)S(1)}, bf16[2,2048,256]{2,1,0:T(8,128)(2,1)}, u32[]{:S(2)}) copy-start(bf16[2,2048,256]{2,1,0:T(8,128)(2,1)} %param.45) | copy-start | bytes 6291460
  150.7 6.4 %copy-start.36 = (f32[16]{0:T(128)S(1)}, f32[16]{0:T(128)}, u32[]{:S(2)}) copy-start(f32[16]{0:T(128)} %get-tuple-element.119) | copy-start | bytes 196
  150.7 25.2 %copy-start.11 = (bf16[256,1024]{1,0:T(8,128)(2,1)S(1)}, bf16[256,1024]{1,0:T(8,128)(2,1)}, u32[]{:S(2)}) copy-start(bf16[256,1024]{1,0:T(8,128)(2,1)} %param.30) | copy-start | bytes 1572868
  153.6 25.0 %copy-start.12 = (bf16[256,512]{1,0:T(8,128)(2,1)S(1)}, bf16[256,512]{1,0:T(8,128)(2,1)}, u32[]{:S(2)}) copy-start(bf16[256,512]{1,0:T(8,128)(2,1)} %param.29) | copy-start | bytes 786436
  153.6 109.0 %all-gather.7.cloned.1.call-start = ((), (), s32[]{:S(2)}) async-start(), calls=%async_computation.2 | async-start | bytes 2621440 | tf_op jit(solution)/shard_map/all_gather | solution.py:203
  193.1 5.1 %copy-start.31 = (f32[1024]{0:T(1024)S(1)}, f32[1024]{0:T(1024)}, u32[]{:S(2)}) copy-start(f32[1024]{0:T(1024)} %param.38) | copy-start | bytes 12292
  227.9 5.2 %copy-start.17 = (s32[256,4]{0,1:T(4,128)S(1)}, s32[256,4]{0,1:T(4,128)}, u32[]{:S(2)}) copy-start(s32[256,4]{0,1:T(4,128)} %param.42) | copy-start | bytes 12292
  227.9 5.4 %copy-start.32 = (f32[256,4]{0,1:T(4,128)S(1)}, f32[256,4]{0,1:T(4,128)}, u32[]{:S(2)}) copy-start(f32[256,4]{0,1:T(4,128)} %param.43) | copy-start | bytes 12292
  227.9 5.6 %copy-start.3 = (bf16[256,2048]{1,0:T(8,128)(2,1)S(1)}, bf16[256,2048]{1,0:T(8,128)(2,1)}, u32[]{:S(2)}) copy-start(bf16[256,2048]{1,0:T(8,128)(2,1)} %copy-done.2) | copy-start | bytes 3145732
  227.9 42.9 %all-to-all-start.1 = ((bf16[2,768,512]{2,0,1:T(2,128)(2,1)}), bf16[2,768,512]{2,0,1:T(2,128)(2,1)}, u32[]{:S(2)}, u32[]{:S(2)}) async-start(bf16[2,768,512]{2,0,1:T(2,128)(2,1)} %copy.125), calls=%async_computation.1 | async-start | bytes 3145728 | tf_op jit(solution)/shard_map/all_to_all | solution.py:213
  235.3 21.0 %copy-start.21 = (s32[1024,1]{0,1:T(1,128)S(1)}, s32[1024,1]{0,1:T(1,128)}, u32[]{:S(2)}) copy-start(s32[1024,1]{0,1:T(1,128)} %copy-done.20) | copy-start | bytes 12292
  (23 other events, 60.7 us)
Sparse Core Ops, SparseCore 0:
  76.0 68.8 all-gather.8
  147.0 29.4 all-gather.12
  178.3 43.1 all-gather.10
  223.2 39.3 all-gather.6
where the time goes:
time: 294 us; the launch traced here: 293 us
  blocking collectives  81.7 us (28%)
  waiting for transfers between devices  69.8 us (24%)
  local copies, waits for them, and re-layouts  55.5 us (19%)
  matrix products  32.9 us (11%)
  other arithmetic  30 us (10%)
  between operations  15.1 us (5%)
  starting transfers between devices  7.51 us (3%)
    all_to_all x1, blocking collectives, on_device(): lax.all_to_all(my_columns, 'ep', split_axis=0, concat_axis=1, tiled=True)  43.9 us
    all_gather x1, waiting for transfers between devices, on_device(): column_piece = lax.all_gather(arrived, 'tp', axis=2, tiled=True)  38.1 us
    all_gather x1, waiting for transfers between devices, on_device(): lax.all_gather(hidden, 'tp', axis=2, tiled=True)  21.9 us
    all_gather x1, blocking collectives, on_device(): lax.all_gather(shared_hidden, 'tp', axis=1, tiled=True)  20.6 us
    unnamed x1, blocking collectives  17.1 us
    unnamed x89, local copies, waits for them, and re-layouts  7.6 us
    gather x1, local copies, waits for them, and re-layouts, on_device(): jnp.take(padded, slot_owner, axis=0).reshape(experts, capacity, model_width)  7.02 us
    gather x2, local copies, waits for them, and re-layouts, on_device(): jnp.take(returned.reshape(experts * capacity, col_width), slot_index, axi...  6.73 us
  transfers between devices with their start and end apart: 6, of which 4 were waited for; matrix products, arithmetic and copies ran while one was open for 26% of the time, Pallas kernels for 0%

commit v1 on v0

--- a/solution.py
+++ b/solution.py
@@ -1,3 +1,4 @@
+import functools
 import jax
 import jax.numpy as jnp
 from jax import lax
@@ -10,6 +11,22 @@
 TOP_K = 4
 epsilon = 1e-05
 precise = lax.Precision.HIGHEST
+
+
+def mix_samples_over_axis(load, pos_dim, array_dim):
+    t_next = jnp.concatenate(
+        lax.all_to_all(
+            jnp.stack(jnp.split(load, lax.axis_size("ep"), pos_dim), axis=0),
+            axis_name="ep",
+            split_axis=0,
+            concat_axis=0,
+        ),
+        array_dim,
+    )
+    return t_next
+
+
+_mix_plate = functools.partial(mix_samples_over_axis, pos_dim=0, array_dim=1)
 
 
 def passed_along(x, axis, by):
@@ -186,7 +203,7 @@
     padded = jnp.concatenate([normed, jnp.zeros((1, model_width), jnp.bfloat16)], axis=0)
     outgoing = jnp.take(padded, slot_owner, axis=0).reshape(experts, capacity, model_width)
     my_columns = lax.dynamic_slice_in_dim(outgoing, lax.axis_index("tp") * col_width, col_width, 2)
-    arrived = lax.all_to_all(my_columns, "ep", split_axis=0, concat_axis=1, tiled=True)
+    arrived = _mix_plate(my_columns)
     column_piece = lax.all_gather(arrived, "tp", axis=2, tiled=True)
     gate_pre = jnp.einsum(
         "esd,edf->esf", column_piece, routed_gate_weight, preferred_element_type=jnp.float32

time: 294 us -> 294 us (level)
    unnamed x89 -> x96, local copies, waits for them, and re-layouts: 7.6 us -> 7.71 us
where the time goes in v1:
time: 294 us; the launch traced here: 293 us
  blocking collectives  81.7 us (28%)
  waiting for transfers between devices  69.8 us (24%)
  local copies, waits for them, and re-layouts  55.6 us (19%)
  matrix products  32.9 us (11%)
  other arithmetic  30 us (10%)
  between operations  15.2 us (5%)
  starting transfers between devices  7.48 us (3%)
    all_to_all x1, blocking collectives, mix_samples_over_axis(): lax.all_to_all(jnp.stack(jnp.split(load, lax.axis_size('ep'), pos_dim), a...  43.9 us
    all_gather x1, waiting for transfers between devices, on_device(): column_piece = lax.all_gather(arrived, 'tp', axis=2, tiled=True)  38.1 us
    all_gather x1, waiting for transfers between devices, on_device(): lax.all_gather(hidden, 'tp', axis=2, tiled=True)  21.9 us
    all_gather x1, blocking collectives, on_device(): lax.all_gather(shared_hidden, 'tp', axis=1, tiled=True)  20.6 us
    unnamed x1, blocking collectives  17.2 us
    unnamed x96, local copies, waits for them, and re-layouts  7.71 us
    gather x1, local copies, waits for them, and re-layouts, on_device(): jnp.take(padded, slot_owner, axis=0).reshape(experts, capacity, model_width)  7.02 us
    gather x2, local copies, waits for them, and re-layouts, on_device(): jnp.take(returned.reshape(experts * capacity, col_width), slot_index, axi...  6.73 us
  transfers between devices with their start and end apart: 6, of which 4 were waited for; matrix products, arithmetic and copies ran while one was open for 26% of the time, Pallas kernels for 0%

profile of v1, /device:TPU:0, one launch (start us, length us, event | category | flops | bytes accessed | tf_op | source)
XLA Modules:
  0.0 292.8 jit_solution(6314324733362054698)
XLA Ops:
  9.2 4.5 %reduce-window.6 = s32[16,8,128]{2,1,0:T(8,128)S(1)} reduce-window(s32[16,8,128]{2,1,0:T(8,128)S(1)} %fusion.58, s32[]{:T(128)} %constant.114.clone.1), window={size=1x1x128 pad=0_0x0_0x127_0}, to_apply=%region_8.9 | reduce-window | flops 2080768 | bytes 131076 | tf_op jit(solution)/shard_map/reduce-window
  15.6 4.3 %scatter_custom_fusion = s32[1536]{0:T(1024)S(1)} fusion(s32[1024]{0:T(1024)S(1)} %bitcast.172, s32[1024]{0:T(1024)S(1)} %add_select_fusion, s32[]{:T(128)} %constant.122.clone.1), kind=kCustom, calls=%fused_computation.121 | custom fusion | bytes 6148 | tf_op jit(solution)/shard_map/scatter | solution.py:89
  21.7 7.0 %gather_fusion = bf16[1536,2048]{1,0:T(8,128)(2,1)} fusion(bf16[257,2048]{1,0:T(8,128)(2,1)S(1)} %concatenate.19, s32[2048]{0:T(1024)S(1)} %pad_clamp_fusion), kind=kCustom, calls=%fused_computation | custom fusion | bytes 12589056 | tf_op jit(solution)/shard_map/jit(_take)/gather | solution.py:204
  30.8 43.9 %all_to_all.20 = bf16[8,2,96,512]{3,2,1,0:T(8,128)(2,1)S(1)} all-to-all(bf16[8,2,96,512]{3,2,1,0:T(8,128)(2,1)S(1)} %fusion.47), channel_id=1, replica_groups=mesh['ep'=8,'tp'=4] {'ep'}, dimensions={0} | all-to-all | bytes 3145728 | tf_op jit(solution)/shard_map/all_to_all | solution.py:18
  95.6 2.9 broadcast_multiply_fusion
  98.7 3.1 %fusion.26 = f32[2,16,64,128]{3,2,1,0:T(8,128)} fusion(f32[2,128,16,128]{3,1,2,0:T(8,128)S(1)} %bitcast.155, f32[2,128,16,64]{1,0,3,2:T(2,128)S(1)} %get-tuple-element.115), kind=kOutput, calls=%fused_computation.43 | convolution fusion | flops 402653184 | bytes 4194304 | tf_op jit(solution)/shard_map/bjhn,bjh,bjhp->bhpn/dot_general | solution.py:162
  101.8 4.1 %while.26 = (s32[]{:T(128)}, f32[16,64,128]{2,1,0:T(8,128)S(1)}, f32[2,16,64,128]{3,2,1,0:T(8,128)}, f32[2,16]{1,0:T(2,128)S(1)}, f32[2,16,64,128]{3,2,1,0:T(8,128)}, /*index=5*/s32[]{:T(128)}, s32[]{:T(128)}) while((s32[]{:T(128)}, f32[16,64,128]{2,1,0:T(8,128)S(1)}, f32[2,16,64,128]{3,2,1,0:T(8,128)}, f32[2,16]{1,0:T(2,128)S(1)}, ...), condition=%wide.region_2.3_spmd.clone, body=%wide.region_1.2_spmd.clone.sunk | while | flops 524291 | bytes 2622240 | solution.py:164
  106.9 38.1 %all-gather.9.cloned.1.call-done = bf16[2,768,2048]{2,1,0:T(8,128)(2,1)} async-done(((bf16[2,768,512]{2,1,0:T(8,128)(2,1)}), bf16[2,768,2048]{2,1,0:T(8,128)(2,1)}) %all-gather.9.cloned.1.call-update) | async-done | bytes 6291472 | tf_op jit(solution)/shard_map/all_gather | solution.py:207
  145.0 5.3 %fusion.70 = f32[2,768,256]{2,1,0:T(8,128)S(1)} fusion(bf16[2,768,2048]{2,1,0:T(8,128)(2,1)} %all-gather.9.cloned.1.call-done, bf16[2,2048,256]{2,1,0:T(8,128)(2,1)} %param.44), kind=kOutput, calls=%fused_computation.139 | convolution fusion | flops 1610612736 | bytes 9961472 | tf_op jit(solution)/shard_map/esd,edf->esf/dot_general | solution.py:208
  150.8 2.9 multiply_convert_fusion
  157.5 17.2 %all-reduce.1 = bf16[128]{0:T(256)(128)(2,1)S(1)} all-reduce(bf16[128]{0:T(256)(128)(2,1)S(1)} %dynamic-update-slice), channel_id=2, replica_groups=mesh['ep'=8,'tp'=4] {'ep'}, use_global_device_ids=true, to_apply=%add.1 | all-reduce | flops 128 | bytes 512
  181.8 4.2 %fusion.16 = f32[2,128,16,64]{1,3,2,0:T(8,128)S(1)} fusion(f32[2,128,16,128]{3,1,2,0:T(8,128)S(1)} %bitcast.156, f32[2,16,64,128]{3,2,1,0:T(8,128)S(1)} %copy-done.9, f32[2,128,16]{1,2,0:T(8,128)S(1)} %copy-done.14, f32[16,64,128]{2,1,0:T(8,128)S(1)} %get-tuple-element.76, f32[2,16]{1,0:T(2,128)S(1)} %copy-done.33), kind=kOutput, calls=%fused_computation.27 | convolution fusion | flops 403439616 | bytes 4735104 | tf_op jit(solution)/shard_map/bihn,bhpn->bihp/dot_general | solution.py:176
  187.3 4.3 %fusion.13 = f32[2,128,16,64]{1,3,2,0:T(8,128)S(1)} fusion(f32[2,128,16,64]{1,3,2,0:T(8,128)S(1)} %fusion.16, f32[2,16,128,128]{3,2,1,0:T(8,128)S(1)} %bitcast.154, f32[2,128,16,64]{1,0,3,2:T(2,128)S(1)} %copy-done.6, f32[2,16,128]{2,1,0:T(8,128)S(1)} %copy.119, pred[128,128]{1,0:T(8,128)(4,1)S(1)} %copy-done.13), kind=kOutput, calls=%fused_computation.25 | convolution fusion | flops 405012480 | bytes 5275648 | tf_op jit(solution)/shard_map/bhij,bjhp->bihp/dot_general | solution.py:157
  193.3 3.1 %reshape.210 = f32[256,4,256]{0,2,1:T(8,128)} reshape(f32[2,128,16,64]{1,0,3,2:T(2,128)} %copy.127) | data formatting | bytes 2097152 | tf_op jit(solution)/shard_map/reshape | solution.py:179
  199.8 21.9 %all-gather.11.cloned.1.call-done = bf16[2,768,1024]{2,1,0:T(8,128)(2,1)} async-done(((bf16[2,768,256]{2,1,0:T(8,128)(2,1)}), bf16[2,768,1024]{2,1,0:T(8,128)(2,1)}) %all-gather.11.cloned.1.call-update) | async-done | bytes 3145744 | tf_op jit(solution)/shard_map/all_gather | solution.py:221
  221.7 3.7 %convolution_convert_fusion = bf16[2,768,512]{2,1,0:T(8,128)(2,1)S(1)} fusion(bf16[2,768,1024]{2,1,0:T(8,128)(2,1)} %all-gather.11.cloned.1.call-done, bf16[2,1024,512]{2,1,0:T(8,128)(2,1)S(1)} %copy-done), kind=kOutput, calls=%fused_computation.21 | convolution fusion | flops 1611399168 | bytes 6815744 | tf_op jit(solution)/shard_map/esf,efd->esd/dot_general | solution.py:227
  228.1 5.0 %all-to-all-start.1 = ((bf16[2,768,512]{2,0,1:T(2,128)(2,1)}), bf16[2,768,512]{2,0,1:T(2,128)(2,1)}, u32[]{:S(2)}, u32[]{:S(2)}) async-start(bf16[2,768,512]{2,0,1:T(2,128)(2,1)} %copy.138), calls=%async_computation.1 | async-start | bytes 3145728 | tf_op jit(solution)/shard_map/all_to_all | solution.py:230
  235.9 20.6 %all_gather.28 = bf16[256,1024]{1,0:T(8,128)(2,1)} all-gather(bf16[256,256]{1,0:T(8,128)(2,1)S(1)} %fusion.18), channel_id=1, replica_groups=mesh['ep'=8,'tp'=4] {'tp'}, dimensions={1}, use_global_device_ids=true | all-gather | bytes 655360 | tf_op jit(solution)/shard_map/all_gather | solution.py:222
  256.5 6.2 %all-gather.7.cloned.1.call-done = bf16[256,4096]{0,1:T(8,128)(2,1)} async-done(((bf16[256,1024]{0,1:T(8,128)(2,1)}), bf16[256,4096]{0,1:T(8,128)(2,1)}) %all-gather.7.cloned.1.call-update) | async-done | bytes 2097168 | tf_op jit(solution)/shard_map/all_gather | solution.py:220
  262.8 4.8 %convolution_convert_fusion.1 = bf16[256,512]{1,0:T(8,128)(2,1)} fusion(bf16[256,4096]{0,1:T(8,128)(2,1)} %all-gather.7.cloned.1.call-done, bf16[4096,512]{1,0:T(8,128)(2,1)} %param.39), kind=kOutput, calls=%fused_computation.32 | convolution fusion | flops 1073872896 | bytes 6553600 | tf_op jit(solution)/shard_map/dot_general | solution.py:224
  267.5 3.4 %all-to-all-done.1 = bf16[2,768,512]{2,0,1:T(2,128)(2,1)} async-done(((bf16[2,768,512]{2,0,1:T(2,128)(2,1)}), bf16[2,768,512]{2,0,1:T(2,128)(2,1)}, u32[]{:S(2)}, u32[]{:S(2)}) %all-to-all-start.1) | async-done | bytes 1572896 | tf_op jit(solution)/shard_map/all_to_all | solution.py:230
  271.0 2.9 copy.139
  273.9 5.6 %gather_fusion.1 = bf16[1024,512]{1,0:T(8,128)(2,1)S(1)} fusion(bf16[1536,512]{1,0:T(8,128)(2,1)} %bitcast.151, s32[1024]{0:T(1024)S(1)} %broadcast_clamp_fusion), kind=kCustom, calls=%fused_computation.1 | custom fusion | bytes 2101248 | tf_op jit(solution)/shard_map/jit(_take)/gather | solution.py:231
  280.6 3.4 %multiply_reduce_fusion = f32[256,512]{1,0:T(8,128)S(1)} fusion(f32[256,4]{1,0:T(8,128)S(1)} %copy.140, bf16[256,4,512]{2,1,0:T(4,128)(2,1)} %gather.15, pred[256,4]{1,0:T(8,128)(4,1)S(1)} %copy.135), kind=kLoop, calls=%fused_computation.14 | loop fusion | flops 1966080 | bytes 1577984 | tf_op jit(solution)/shard_map/reduce_sum | solution.py:233
  (201 shorter events, 59.2 us)
Async XLA Ops:
  7.2 214.5 %copy-start = (bf16[2,1024,512]{2,1,0:T(8,128)(2,1)S(1)}, bf16[2,1024,512]{2,1,0:T(8,128)(2,1)}, u32[]{:S(2)}) copy-start(bf16[2,1024,512]{2,1,0:T(8,128)(2,1)} %param.46) | copy-start | bytes 6291460
  7.2 12.8 %copy-start.7 = (bf16[256,2048]{1,0:T(8,128)(2,1)S(1)}, bf16[256,2048]{1,0:T(8,128)(2,1)}, u32[]{:S(2)}) copy-start(bf16[256,2048]{1,0:T(8,128)(2,1)} %param.40) | copy-start | bytes 3145732
  7.2 13.2 %copy-start.25 = (f32[2048]{0:T(1024)S(1)}, f32[2048]{0:T(1024)}, u32[]{:S(2)}) copy-start(f32[2048]{0:T(1024)} %param.41) | copy-start | bytes 24580
  7.2 137.8 %all-gather.9.cloned.1.call-start = ((), (), s32[]{:S(2)}) async-start(), calls=%async_computation.3 | async-start | bytes 7864320 | tf_op jit(solution)/shard_map/all_gather | solution.py:207
  74.7 6.0 %copy-start.40 = (f32[16]{0:T(128)S(1)}, f32[16]{0:T(128)}, u32[]{:S(2)}) copy-start(f32[16]{0:T(128)} %param.33) | copy-start | bytes 196
  74.7 6.0 %copy-start.23 = (f32[256,16]{0,1:T(8,128)S(1)}, f32[256,16]{0,1:T(8,128)}, u32[]{:S(2)}) copy-start(f32[256,16]{0,1:T(8,128)} %param.31) | copy-start | bytes 49156
  74.7 6.0 %copy-start.24 = (f32[256,16]{0,1:T(8,128)S(1)}, f32[256,16]{0,1:T(8,128)}, u32[]{:S(2)}) copy-start(f32[256,16]{0,1:T(8,128)} %param.32) | copy-start | bytes 49156
  76.0 6.3 %copy-start.30 = (f32[4,512]{1,0:T(4,128)S(1)}, f32[4,512]{1,0:T(4,128)}, u32[]{:S(2)}) copy-start(f32[4,512]{1,0:T(4,128)} %param.36) | copy-start | bytes 24580
  76.0 6.9 %copy-start.22 = (f32[4,1024]{1,0:T(4,128)S(1)}, f32[4,1024]{1,0:T(4,128)}, u32[]{:S(2)}) copy-start(f32[4,1024]{1,0:T(4,128)} %param.35) | copy-start | bytes 49156
  76.0 104.3 %all-gather.13.cloned.1.call-start = ((), (), s32[]{:S(2)}) async-start(), calls=%async_computation.5 | async-start | bytes 2359296 | tf_op jit(solution)/shard_map/all_gather | solution.py:41
  78.6 7.2 %collective-permute-start = (bf16[3,2048]{0,1:T(8,128)(2,1)}, bf16[3,2048]{0,1:T(8,128)(2,1)}, u32[]{:S(2)}, u32[]{:S(2)}) collective-permute-start(bf16[3,2048]{0,1:T(8,128)(2,1)} %copy.111), channel_id=1, source_target_pairs={{0,4},{4,8},{8,12},{12,16},{16,20},{20,24},{24,28},{1,5},{5,9},{9,... | collective-permute-start | bytes 36872 | tf_op jit(solution)/shard_map/ppermute | solution.py:35
  106.7 115.0 %all-gather.11.cloned.1.call-start = ((), (), s32[]{:S(2)}) async-start(), calls=%async_computation.4 | async-start | bytes 3932160 | tf_op jit(solution)/shard_map/all_gather | solution.py:221
  145.0 5.4 %copy-start.37 = (bf16[2,768,2048]{2,1,0:T(8,128)(2,1)S(1)}, bf16[2,768,2048]{2,1,0:T(8,128)(2,1)}, u32[]{:S(2)}) copy-start(bf16[2,768,2048]{2,1,0:T(8,128)(2,1)} %all-gather.9.cloned.1.call-done) | copy-start | bytes 18874372
  145.0 5.8 %copy-start.38 = (bf16[2,2048,256]{2,1,0:T(8,128)(2,1)S(1)}, bf16[2,2048,256]{2,1,0:T(8,128)(2,1)}, u32[]{:S(2)}) copy-start(bf16[2,2048,256]{2,1,0:T(8,128)(2,1)} %param.45) | copy-start | bytes 6291460
  150.8 6.4 %copy-start.36 = (f32[16]{0:T(128)S(1)}, f32[16]{0:T(128)}, u32[]{:S(2)}) copy-start(f32[16]{0:T(128)} %get-tuple-element.119) | copy-start | bytes 196
  150.8 25.2 %copy-start.11 = (bf16[256,1024]{1,0:T(8,128)(2,1)S(1)}, bf16[256,1024]{1,0:T(8,128)(2,1)}, u32[]{:S(2)}) copy-start(bf16[256,1024]{1,0:T(8,128)(2,1)} %param.30) | copy-start | bytes 1572868
  153.8 25.0 %copy-start.12 = (bf16[256,512]{1,0:T(8,128)(2,1)S(1)}, bf16[256,512]{1,0:T(8,128)(2,1)}, u32[]{:S(2)}) copy-start(bf16[256,512]{1,0:T(8,128)(2,1)} %param.29) | copy-start | bytes 786436
  153.8 109.0 %all-gather.7.cloned.1.call-start = ((), (), s32[]{:S(2)}) async-start(), calls=%async_computation.2 | async-start | bytes 2621440 | tf_op jit(solution)/shard_map/all_gather | solution.py:220
  193.3 5.1 %copy-start.31 = (f32[1024]{0:T(1024)S(1)}, f32[1024]{0:T(1024)}, u32[]{:S(2)}) copy-start(f32[1024]{0:T(1024)} %param.38) | copy-start | bytes 12292
  228.1 5.2 %copy-start.17 = (s32[256,4]{0,1:T(4,128)S(1)}, s32[256,4]{0,1:T(4,128)}, u32[]{:S(2)}) copy-start(s32[256,4]{0,1:T(4,128)} %param.42) | copy-start | bytes 12292
  228.1 5.4 %copy-start.32 = (f32[256,4]{0,1:T(4,128)S(1)}, f32[256,4]{0,1:T(4,128)}, u32[]{:S(2)}) copy-start(f32[256,4]{0,1:T(4,128)} %param.43) | copy-start | bytes 12292
  228.1 5.5 %copy-start.3 = (bf16[256,2048]{1,0:T(8,128)(2,1)S(1)}, bf16[256,2048]{1,0:T(8,128)(2,1)}, u32[]{:S(2)}) copy-start(bf16[256,2048]{1,0:T(8,128)(2,1)} %copy-done.2) | copy-start | bytes 3145732
  228.1 42.9 %all-to-all-start.1 = ((bf16[2,768,512]{2,0,1:T(2,128)(2,1)}), bf16[2,768,512]{2,0,1:T(2,128)(2,1)}, u32[]{:S(2)}, u32[]{:S(2)}) async-start(bf16[2,768,512]{2,0,1:T(2,128)(2,1)} %copy.138), calls=%async_computation.1 | async-start | bytes 3145728 | tf_op jit(solution)/shard_map/all_to_all | solution.py:230
  235.4 21.1 %copy-start.21 = (s32[1024,1]{0,1:T(1,128)S(1)}, s32[1024,1]{0,1:T(1,128)}, u32[]{:S(2)}) copy-start(s32[1024,1]{0,1:T(1,128)} %copy-done.20) | copy-start | bytes 12292
  (23 other events, 60.7 us)
Sparse Core Ops, SparseCore 0:
  76.2 68.8 all-gather.8
  147.2 29.4 all-gather.12
  178.5 43.0 all-gather.10
  223.4 39.3 all-gather.6
